TPU v7x, 32 devices: a whole 2x2x4 slice. The times are simulated.
32 devices in a mesh: sp: 8 (over z, x), tp: 4 (over y, core).
Axes of the slice: x: 2, y: 2, z: 4, core: 2. Of those that a mesh axis runs over, the one named last changes fastest.
Arguments:
- residual_in: bfloat16 [2048, 2048], P('sp', 'tp'), may hold values from -6 to 6
- conv_input: bfloat16 [2048, 512], P('sp', 'tp'), may hold values from -6 to 6
- outer_gate: bfloat16 [2048, 512], P('sp', 'tp'), may hold values from -6 to 6
- inner_gate: bfloat16 [2048, 512], P('sp', 'tp'), may hold values from -6 to 6
- documents: int32 [2048], P('sp'), may hold values from 0 to 3, as said below
- conv_taps: float32 [3, 512], P(None, 'tp'), may hold values from -3 to 3
- mixer_gain: float32 [512], replicated, may hold values from 0.1 to 1.9
- output_weight: bfloat16 [512, 2048], P(None, 'tp'), may hold values from -0.25 to 0.25
- ffn_gain: float32 [2048], P('tp'), may hold values from 0.1 to 1.9
- routes: int32 [2048, 2], P('sp'), may hold values from 0 to 7, all different within a row; in each aligned block of 256 rows (0 to 255, 256 to 511, ...) at most 128 rows name the same one
- route_weights: float32 [2048, 2], P('sp'), may hold values from 0.1 to 0.9
- expert_gate: bfloat16 [8, 2048, 3584], P('sp', None, 'tp'), may hold values from -0.125 to 0.125
- expert_up: bfloat16 [8, 2048, 3584], P('sp', None, 'tp'), may hold values from -0.125 to 0.125
- expert_down: bfloat16 [8, 3584, 2048], P('sp', 'tp'), may hold values from -0.09375 to 0.09375
Outputs:
- layer_out: bfloat16 [2048, 2048], P('sp', 'tp')
Inputs may be any that keep to these rules, and one draw needn't show every extreme that they name: Document numbers never fall along the positions, and each of the 4 documents occurs. Every document has 256 to 768 positions, and one has exactly 768. `routes`: the two experts of a position differ. Among the 256 positions of one index of sp no expert is named more than 128 times, a bound that some block reaches.
All inputs are finite; a program needn't handle non-finite values.
Results may differ from a plain program's by a relative error of at most 0.0058.
Values may be sent and summed in bfloat16 or wider, within the bound.
A program may use at most 64 MiB of HBM per device.

v0:
```python
import jax
import jax.numpy as jnp
from jax import lax
from jax.sharding import PartitionSpec as P

EPS = 1e-06


def from_behind(block, axis, distance):
    devices = range(lax.axis_size(axis))
    route = [(i - distance, i) for i in devices if i - distance in devices]
    return lax.ppermute(block, axis, route)


def slot_tables(routes, experts, capacity):
    tokens = routes.shape[0]
    flattened = routes.reshape(-1)
    onehot = (flattened[:, None] == jnp.arange(experts, dtype=jnp.int32)[None, :]).astype(jnp.int32)
    earlier = jnp.cumsum(onehot, axis=0) - onehot
    position_in = jnp.sum(earlier * onehot, axis=1)
    target = flattened * capacity + position_in
    owners = (
        jnp.full((experts * capacity,), tokens, jnp.int32)
        .at[target]
        .set(jnp.arange(2 * tokens, dtype=jnp.int32) // 2)
    )
    return (target, owners)


def per_device(
    residual_in,
    conv_input,
    outer_gate,
    inner_gate,
    documents,
    conv_taps,
    mixer_gain,
    output_weight,
    ffn_gain,
    routes,
    route_weights,
    expert_gate,
    expert_up,
    expert_down,
):
    tokens_here = residual_in.shape[0]
    local_features = residual_in.shape[1]
    conv_value = (inner_gate.astype(jnp.float32) * conv_input.astype(jnp.float32)).astype(
        jnp.bfloat16
    )
    doc_marks = documents.astype(jnp.bfloat16)
    before_rows, before_docs = from_behind((conv_value[-2:], doc_marks[-2:]), "sp", 1)
    joined_rows = jnp.concatenate([before_rows, conv_value], axis=0).astype(jnp.float32)
    joined_docs = jnp.concatenate([before_docs, doc_marks], axis=0)
    same_one = (joined_docs[1:-1] == doc_marks).astype(jnp.float32)[:, None]
    same_two = (joined_docs[:-2] == doc_marks).astype(jnp.float32)[:, None]
    conv_sum = (
        conv_taps[2] * joined_rows[2:]
        + conv_taps[1] * joined_rows[1:-1] * same_one
        + conv_taps[0] * joined_rows[:-2] * same_two
    )
    mixed = (outer_gate.astype(jnp.float32) * conv_sum).astype(jnp.bfloat16)
    piece_f = lax.all_gather(mixed, "tp", axis=1, tiled=True).astype(jnp.float32)
    scaled = (piece_f * mixer_gain).astype(jnp.bfloat16)
    accum = jnp.dot(scaled, output_weight, preferred_element_type=jnp.float32)
    squares = jnp.sum(piece_f * piece_f, axis=1)
    mix_scale = lax.rsqrt(squares / mixer_gain.shape[0] + EPS)
    hidden_state = residual_in.astype(jnp.float32) + accum * mix_scale[:, None]
    feature_total = lax.psum(jnp.sum(hidden_state * hidden_state, axis=1), "tp")
    model_width = local_features * lax.axis_size("tp")
    normed = (
        hidden_state * lax.rsqrt(feature_total / model_width + EPS)[:, None] * ffn_gain
    ).astype(jnp.bfloat16)
    experts = lax.axis_size("sp") * expert_gate.shape[0]
    capacity = 4 * tokens_here // experts
    target, owners = slot_tables(routes, experts, capacity)
    padded = jnp.concatenate([normed, jnp.zeros((1, local_features), jnp.bfloat16)], axis=0)
    outgoing = padded[owners].reshape(experts, capacity, local_features)
    slices_in = lax.all_to_all(outgoing, "sp", split_axis=0, concat_axis=0, tiled=True)
    arrived = lax.all_gather(slices_in, "tp", axis=2, tiled=True)
    expert_in = arrived.reshape(-1, model_width)
    gate = jnp.dot(expert_in, expert_gate[0], preferred_element_type=jnp.float32)
    upper = jnp.dot(expert_in, expert_up[0], preferred_element_type=jnp.float32)
    act = (jax.nn.silu(gate) * upper).astype(jnp.bfloat16)
    partial_out = jnp.dot(act, expert_down[0], preferred_element_type=jnp.float32)
    summed = lax.psum_scatter(
        partial_out.astype(jnp.bfloat16), "tp", scatter_dimension=1, tiled=True
    )
    returned = lax.all_to_all(
        summed.reshape(experts, capacity, local_features),
        "sp",
        split_axis=0,
        concat_axis=0,
        tiled=True,
    )
    picked = returned.reshape(experts * capacity, local_features)[target].astype(jnp.float32)
    picked = picked.reshape(tokens_here, 2, local_features)
    routed = jnp.sum(picked * route_weights[:, :, None], axis=1)
    return (hidden_state + routed).astype(jnp.bfloat16)


def solution(mesh):
    placed = (
        P("sp", "tp"),
        P("sp", "tp"),
        P("sp", "tp"),
        P("sp", "tp"),
        P("sp"),
        P(None, "tp"),
        P(),
        P(None, "tp"),
        P("tp"),
        P("sp", None),
        P("sp", None),
        P("sp", None, "tp"),
        P("sp", None, "tp"),
        P("sp", "tp", None),
    )
    return jax.shard_map(
        per_device, mesh=mesh, in_specs=placed, out_specs=P("sp", "tp"), check_vma=False
    )
```

profile of v0, /device:TPU:0, one launch (start us, length us, event | category | flops | bytes accessed | tf_op | source)
XLA Modules:
  0.0 212.3 jit_solution(1286813573739635724)
XLA Ops:
  6.5 0.0 copy-start
  6.5 0.0 all-gather.2.cloned.1.call-start
  6.5 0.7 convert_element_type.68
  7.3 0.1 slice.41
  7.4 4.9 %collective-permute-start.1 = (bf16[2]{0:T(256)(128)(2,1)S(1)}, bf16[2]{0:T(256)(128)(2,1)S(1)}, u32[]{:S(2)}, u32[]{:S(2)}) collective-permute-start(bf16[2]{0:T(256)(128)(2,1)S(1)} %slice.41), channel_id=1, source_target_pairs={{0,4},{4,8},{8,12},{12,16},{16,20},{20,24},{24,28},{1,5},{5,9},{9,... | collective-permute-start | bytes 20 | tf_op jit(solution)/shard_map/ppermute | solution.py:12
  12.2 0.9 multiply_convert_fusion.2
  13.1 3.5 %collective-permute-start = (bf16[2,128]{1,0:T(2,128)(2,1)S(1)}, bf16[2,128]{1,0:T(2,128)(2,1)S(1)}, u32[]{:S(2)}, u32[]{:S(2)}) collective-permute-start(bf16[2,128]{1,0:T(2,128)(2,1)S(1)} %slice.52), channel_id=1, source_target_pairs={{0,4},{4,8},{8,12},{12,16},{16,20},{20,24},{24,28},{1,5},{5,9},{9,... | collective-permute-start | bytes 1544 | tf_op jit(solution)/shard_map/ppermute | solution.py:12
  16.6 0.8 copy.17
  17.4 0.1 eq.37
  17.6 0.1 eq.33
  17.7 0.7 broadcast_multiply_fusion
  18.4 0.8 slice_bitcast_fusion.2
  19.2 1.1 reduce-window.6
  20.3 0.2 slice_reduce_fusion
  20.6 0.1 copy.16
  20.7 0.1 mul.151
  20.9 0.1 fusion.19
  21.0 2.4 %scatter_custom_fusion = s32[1024]{0:T(1024)S(1)} fusion(s32[512]{0:T(512)S(1)} %bitcast.38, s32[512]{0:T(512)S(1)} %add_select_fusion, s32[]{:T(128)} %constant.38.clone.1), kind=kCustom, calls=%fused_computation.49 | custom fusion | bytes 4100 | tf_op jit(solution)/shard_map/scatter | solution.py:25
  23.5 0.0 collective-permute-done.1
  23.5 0.1 pad_maximum_fusion
  23.6 0.8 compare_convert_fusion.1
  24.3 0.0 collective-permute-done
  24.3 1.0 fusion.15
  25.3 5.8 %all_gather.6 = bf16[256,512]{1,0:T(8,128)(2,1)S(1)} all-gather(bf16[256,128]{1,0:T(8,128)(2,1)S(1)} %fusion.15), channel_id=1, replica_groups=mesh['sp'=8,'tp'=4] {'tp'}, dimensions={1}, use_global_device_ids=true | all-gather | bytes 327680 | tf_op jit(solution)/shard_map/all_gather | solution.py:63
  31.1 0.1 fusion.9
  31.3 1.4 multiply_reduce_fusion.1
  32.7 7.1 %psum.7 = f32[256]{0:T(256)S(1)} all-reduce(f32[256]{0:T(256)S(1)} %get-tuple-element.10), channel_id=1, replica_groups=mesh['sp'=8,'tp'=4] {'tp'}, use_global_device_ids=true, to_apply=%region_2.0 | all-reduce | flops 256 | bytes 2048 | tf_op jit(solution)/shard_map/psum | solution.py:69
  39.8 0.1 multiply_convert_fusion.1
  39.9 4.0 %gather_fusion = bf16[1024,512]{1,0:T(8,128)(2,1)S(1)} fusion(bf16[257,512]{1,0:T(8,128)(2,1)S(1)} %concatenate.11, s32[1024]{0:T(1024)S(1)} %fusion.21), kind=kCustom, calls=%fused_computation | custom fusion | bytes 2101248 | tf_op jit(solution)/shard_map/gather | solution.py:78
  43.9 29.1 %all_to_all.10 = bf16[8,128,512]{2,1,0:T(8,128)(2,1)} all-to-all(bf16[8,128,512]{2,1,0:T(8,128)(2,1)S(1)} %bitcast.36), channel_id=1, replica_groups=mesh['sp'=8,'tp'=4] {'sp'}, dimensions={0} | all-to-all | bytes 2097152 | tf_op jit(solution)/shard_map/all_to_all | solution.py:79
  73.0 0.0 all-gather.2.cloned.1.call-update
  73.0 0.0 reduce-scatter.2.cloned.1.call-start
  73.1 33.6 %all-gather.2.cloned.1.call-done = bf16[8,128,2048]{2,1,0:T(8,128)(2,1)} async-done(((bf16[8,128,512]{2,1,0:T(8,128)(2,1)}), bf16[8,128,2048]{2,1,0:T(8,128)(2,1)}) %all-gather.2.cloned.1.call-update) | async-done | bytes 4194320 | tf_op jit(solution)/shard_map/all_gather | solution.py:80
  106.6 7.5 %fusion.1 = f32[1024,896]{1,0:T(8,128)S(1)} fusion(bf16[1024,2048]{1,0:T(8,128)(2,1)} %bitcast.41, bf16[1,2048,896]{2,1,0:T(8,128)(2,1)} %param.26), kind=kOutput, calls=%fused_computation.5 | convolution fusion | flops 3758096384 | bytes 11534336 | tf_op jit(solution)/shard_map/dot_general | solution.py:83
  114.1 0.0 copy-done.3
  114.1 0.0 copy-done.4
  114.2 0.0 copy-start.5
  114.2 4.8 %multiply_convert_fusion = bf16[1024,896]{1,0:T(8,128)(2,1)S(1)} fusion(f32[1024,896]{1,0:T(8,128)S(1)} %fusion.1, bf16[1024,2048]{1,0:T(8,128)(2,1)S(1)} %bitcast.42, bf16[1,2048,896]{2,1,0:T(8,128)(2,1)S(1)} %copy-done.4), kind=kOutput, calls=%fused_computation.9 | convolution fusion | flops 3763601408 | bytes 13369344 | tf_op jit(solution)/shard_map/dot_general | solution.py:82
  118.9 6.1 %convolution_convert_fusion = bf16[1024,2048]{1,0:T(8,128)(2,1)} fusion(bf16[1024,896]{1,0:T(8,128)(2,1)S(1)} %multiply_convert_fusion, bf16[1,896,2048]{2,1,0:T(8,128)(2,1)S(1)} %copy-done.5), kind=kOutput, calls=%fused_computation.3 | convolution fusion | flops 3760193536 | bytes 9699328 | tf_op jit(solution)/shard_map/dot_general | solution.py:85
  125.0 0.0 reduce-scatter.2.cloned.1.call-update
  125.0 44.6 %reduce-scatter.2.cloned.1.call-done = bf16[1024,512]{1,0:T(8,128)(2,1)} async-done(((bf16[1024,2048]{1,0:T(8,128)(2,1)}), bf16[1024,512]{1,0:T(8,128)(2,1)}) %reduce-scatter.2.cloned.1.call-update) | async-done | bytes 1048592 | tf_op jit(solution)/shard_map/reduce_scatter | solution.py:86
  169.6 5.5 %all-to-all-start.1 = ((bf16[8,128,512]{2,1,0:T(8,128)(2,1)}), bf16[8,128,512]{2,1,0:T(8,128)(2,1)S(1)}, u32[]{:S(2)}, u32[]{:S(2)}) async-start(bf16[8,128,512]{2,1,0:T(8,128)(2,1)} %bitcast.37), calls=%async_computation.2 | async-start | bytes 2097152 | tf_op jit(solution)/shard_map/all_to_all | solution.py:89
  175.1 0.1 copy.19
  175.2 25.5 %all-to-all-done.1 = bf16[8,128,512]{2,1,0:T(8,128)(2,1)S(1)} async-done(((bf16[8,128,512]{2,1,0:T(8,128)(2,1)}), bf16[8,128,512]{2,1,0:T(8,128)(2,1)S(1)}, u32[]{:S(2)}, u32[]{:S(2)}) %all-to-all-start.1) | async-done | bytes 1048608 | tf_op jit(solution)/shard_map/all_to_all | solution.py:89
  200.8 2.0 gather_fusion.1
  202.7 0.7 reshape.78
  203.4 1.3 multiply_reduce_fusion
  204.7 0.8 add_convert_fusion
  (20 shorter events, 0.1 us)
Async XLA Ops:
  6.5 24.8 %copy-start = (bf16[512,512]{1,0:T(8,128)(2,1)S(1)}, bf16[512,512]{1,0:T(8,128)(2,1)}, u32[]{:S(2)}) copy-start(bf16[512,512]{1,0:T(8,128)(2,1)} %param.21) | copy-start | bytes 1572868
  6.5 33.2 %copy-start.1 = (f32[512]{0:T(512)S(1)}, f32[512]{0:T(512)}, u32[]{:S(2)}) copy-start(f32[512]{0:T(512)} %param.22) | copy-start | bytes 6148
  6.5 100.1 %all-gather.2.cloned.1.call-start = ((), (), s32[]{:S(2)}) async-start(), calls=%async_computation.3 | async-start | bytes 5242880 | tf_op jit(solution)/shard_map/all_gather | solution.py:80
  7.4 16.1 %collective-permute-start.1 = (bf16[2]{0:T(256)(128)(2,1)S(1)}, bf16[2]{0:T(256)(128)(2,1)S(1)}, u32[]{:S(2)}, u32[]{:S(2)}) collective-permute-start(bf16[2]{0:T(256)(128)(2,1)S(1)} %slice.41), channel_id=1, source_target_pairs={{0,4},{4,8},{8,12},{12,16},{16,20},{20,24},{24,28},{1,5},{5,9},{9,... | collective-permute-start | bytes 20 | tf_op jit(solution)/shard_map/ppermute | solution.py:12
  13.1 11.2 %collective-permute-start = (bf16[2,128]{1,0:T(2,128)(2,1)S(1)}, bf16[2,128]{1,0:T(2,128)(2,1)S(1)}, u32[]{:S(2)}, u32[]{:S(2)}) collective-permute-start(bf16[2,128]{1,0:T(2,128)(2,1)S(1)} %slice.52), channel_id=1, source_target_pairs={{0,4},{4,8},{8,12},{12,16},{16,20},{20,24},{24,28},{1,5},{5,9},{9,... | collective-permute-start | bytes 1544 | tf_op jit(solution)/shard_map/ppermute | solution.py:12
  73.0 96.6 %reduce-scatter.2.cloned.1.call-start = ((), (), s32[]{:S(2)}) async-start(), calls=%async_computation.4 | async-start | bytes 5242880 | tf_op jit(solution)/shard_map/reduce_scatter | solution.py:86
  106.6 7.5 %copy-start.3 = (bf16[8,128,2048]{2,1,0:T(8,128)(2,1)S(1)}, bf16[8,128,2048]{2,1,0:T(8,128)(2,1)}, u32[]{:S(2)}) copy-start(bf16[8,128,2048]{2,1,0:T(8,128)(2,1)} %all-gather.2.cloned.1.call-done) | copy-start | bytes 12582916
  106.6 7.5 %copy-start.4 = (bf16[1,2048,896]{2,1,0:T(8,128)(2,1)S(1)}, bf16[1,2048,896]{2,1,0:T(8,128)(2,1)}, u32[]{:S(2)}) copy-start(bf16[1,2048,896]{2,1,0:T(8,128)(2,1)} %param.25) | copy-start | bytes 11010052
  114.2 4.8 %copy-start.5 = (bf16[1,896,2048]{2,1,0:T(8,128)(2,1)S(1)}, bf16[1,896,2048]{2,1,0:T(8,128)(2,1)}, u32[]{:S(2)}) copy-start(bf16[1,896,2048]{2,1,0:T(8,128)(2,1)} %param.27) | copy-start | bytes 11010052
  125.0 50.1 %copy-start.2 = (f32[256,2]{0,1:T(2,128)S(1)}, f32[256,2]{0,1:T(2,128)}, u32[]{:S(2)}) copy-start(f32[256,2]{0,1:T(2,128)} %param.24) | copy-start | bytes 6148
  169.6 31.2 %all-to-all-start.1 = ((bf16[8,128,512]{2,1,0:T(8,128)(2,1)}), bf16[8,128,512]{2,1,0:T(8,128)(2,1)S(1)}, u32[]{:S(2)}, u32[]{:S(2)}) async-start(bf16[8,128,512]{2,1,0:T(8,128)(2,1)} %bitcast.37), calls=%async_computation.2 | async-start | bytes 2097152 | tf_op jit(solution)/shard_map/all_to_all | solution.py:89
Sparse Core Ops, SparseCore 0:
  73.1 33.4 all-gather.1
  125.1 44.3 reduce-scatter.1
where the time goes:
time: 213 us; the launch traced here: 212 us
  waiting for transfers between devices  104 us (49%)
  blocking collectives  42 us (20%)
  matrix products  19.7 us (9%)
  starting transfers between devices  13.9 us (7%)
  between operations  13.6 us (6%)
  local copies, waits for them, and re-layouts  11.7 us (5%)
  other arithmetic  7.8 us (4%)
    reduce_scatter x1, waiting for transfers between devices, per_device(): lax.psum_scatter(partial_out.astype(jnp.bfloat16), 'tp', scatter_dimensio...  44.6 us
    all_gather x1, waiting for transfers between devices, per_device(): arrived = lax.all_gather(slices_in, 'tp', axis=2, tiled=True)  33.6 us
    all_to_all x1, blocking collectives, per_device(): lax.all_to_all(outgoing, 'sp', split_axis=0, concat_axis=0, tiled=True)  29.1 us
    all_to_all x1, waiting for transfers between devices, per_device(): lax.all_to_all(summed.reshape(experts, capacity, local_features), 'sp', s...  25.5 us
    ppermute x2, starting transfers between devices, from_behind(): return lax.ppermute(block, axis, route)  8.32 us
    dot_general x1, matrix products, per_device(): upper = jnp.dot(expert_in, expert_up[0], preferred_element_type=jnp.float32)  7.49 us
    psum x1, blocking collectives, per_device(): feature_total = lax.psum(jnp.sum(hidden_state * hidden_state, axis=1), 'tp')  7.09 us
    dot_general x1, matrix products, per_device(): jnp.dot(act, expert_down[0], preferred_element_type=jnp.float32)  6.05 us
  transfers between devices with their start and end apart: 5, of which 3 were waited for; matrix products, arithmetic and copies ran while one was open for 4% of the time, Pallas kernels for 0%

commit v1 on v0

--- a/solution.py
+++ b/solution.py
@@ -1,9 +1,14 @@
+import functools
+
 import jax
 import jax.numpy as jnp
 from jax import lax
+from jax.experimental import pallas as pl
+from jax.experimental.pallas import tpu as pltpu
 from jax.sharding import PartitionSpec as P
 
 EPS = 1e-06
+MESH = pl.DeviceIdType.MESH
 
 
 def from_behind(block, axis, distance):
@@ -25,6 +30,281 @@
         .set(jnp.arange(2 * tokens, dtype=jnp.int32) // 2)
     )
     return (target, owners)
+
+
+def expert_kernel(
+    n,
+    group,
+    out_ref_in,
+    gate_hbm,
+    up_hbm,
+    down_hbm,
+    returned,
+    wg,
+    wu,
+    wd,
+    arrived,
+    act,
+    msend,
+    mrecv,
+    mine,
+    ysend,
+    yrecv,
+    mine2,
+    rsend,
+    w_sem,
+    a2a_s,
+    a2a_r,
+    agy_s,
+    agy_r,
+    agm_s,
+    agm_r,
+    agf_s,
+    agf_r,
+    rsm_s,
+    rsm_r,
+    rsy_s,
+    rsy_r,
+    ret_s,
+    ret_r,
+):
+    outgoing = out_ref_in
+    me = lax.axis_index("sp")
+    t = lax.axis_index("tp")
+    a = t // 2
+    b = t % 2
+    mate = 2 * a + (1 - b)
+    partner = 2 * (1 - a) + b
+    cap, lf = outgoing.shape[1], outgoing.shape[2]
+    hidden = wg.shape[1]
+    rows = group * cap
+    steps = n // group
+
+    loads = [
+        pltpu.make_async_copy(gate_hbm.at[0], wg, w_sem.at[0]),
+        pltpu.make_async_copy(up_hbm.at[0], wu, w_sem.at[1]),
+        pltpu.make_async_copy(down_hbm.at[0], wd, w_sem.at[2]),
+    ]
+    for load in loads:
+        load.start()
+
+    barrier = pltpu.get_barrier_semaphore()
+
+    def greet(p, c):
+        pl.semaphore_signal(
+            barrier, inc=1, device_id={"sp": (me + p) % n}, device_id_type=MESH
+        )
+        return c
+
+    lax.fori_loop(1, n, greet, 0)
+    for other in (mate, partner):
+        pl.semaphore_signal(barrier, inc=1, device_id={"tp": other}, device_id_type=MESH)
+    pl.semaphore_wait(barrier, n + 1)
+
+    def remote(src, dst, s, r, dev):
+        return pltpu.make_async_remote_copy(
+            src_ref=src, dst_ref=dst, send_sem=s, recv_sem=r, device_id=dev, device_id_type=MESH
+        )
+
+    def span(p):
+        return pl.ds(pl.multiple_of(p * cap, cap), cap)
+
+    def span_g(i):
+        return pl.ds(pl.multiple_of(i * rows, rows), rows)
+
+    def a2a(p):
+        return remote(
+            outgoing.at[(me + p) % n],
+            arrived.at[t, span(p)],
+            a2a_s.at[p],
+            a2a_r.at[p],
+            {"sp": (me + p) % n},
+        )
+
+    def slab(p):
+        return arrived.at[t, span(p)]
+
+    def agy(p):
+        return remote(slab(p), slab(p), agy_s.at[p], agy_r.at[p], {"tp": partner})
+
+    def agm(p):
+        return remote(slab(p), slab(p), agm_s.at[p], agm_r.at[p], {"tp": mate})
+
+    def agf(p):
+        piece = arrived.at[partner, span(p)]
+        return remote(piece, piece, agf_s.at[p], agf_r.at[p], {"tp": mate})
+
+    def rsm(i):
+        return remote(msend.at[i], mrecv.at[i], rsm_s.at[i], rsm_r.at[i], {"tp": mate})
+
+    def rsy(i):
+        return remote(ysend.at[i], yrecv.at[i], rsy_s.at[i], rsy_r.at[i], {"tp": partner})
+
+    def ret(p):
+        return remote(
+            rsend.at[span(p)],
+            returned.at[me],
+            ret_s.at[p],
+            ret_r.at[p],
+            {"sp": (me + n - p) % n},
+        )
+
+    def each(low, high, f):
+        def one(p, c):
+            f(p)
+            return c
+
+        lax.fori_loop(low, high, one, 0)
+
+    each(1, n, lambda p: a2a(p).start())
+    arrived[t, pl.ds(0, cap), :] = outgoing[me]
+
+    def spread(p):
+        @pl.when(p > 0)
+        def _():
+            a2a(p).wait_recv()
+
+        agy(p).start()
+        agm(p).start()
+
+    def relay(p):
+        agy(p).wait_recv()
+        agf(p).start()
+
+    def settle(p):
+        agm(p).wait_recv()
+        agf(p).wait_recv()
+
+    def over_group(i, f):
+        each(i * group, (i + 1) * group, f)
+
+    def reduce_mate(i):
+        rsm(i).wait_recv()
+        ysend[i] = (mine[1 - a] + mrecv[i, 1 - a].astype(jnp.float32)).astype(jnp.bfloat16)
+        rsy(i).start()
+        mine2[...] = mine[a] + mrecv[i, a].astype(jnp.float32)
+
+    def reduce_partner(i):
+        rsy(i).wait_recv()
+        rsend[span_g(i), :] = (mine2[...] + yrecv[i].astype(jnp.float32)).astype(jnp.bfloat16)
+
+        def back(p):
+            @pl.when(p > 0)
+            def _():
+                ret(p).start()
+
+        over_group(i, back)
+
+    def compute(i):
+        def hidden_tile(j, c):
+            cols = pl.ds(pl.multiple_of(j * 128, 128), 128)
+            both = None
+            for q in range(4):
+                deep = slice(q * lf, (q + 1) * lf)
+                w = jnp.concatenate([wg[deep, cols], wu[deep, cols]], axis=1)
+                part = jnp.dot(arrived[q, span_g(i), :], w, preferred_element_type=jnp.float32)
+                both = part if both is None else both + part
+            g = both[:, :128]
+            act[:, cols] = (g * jax.nn.sigmoid(g) * both[:, 128:]).astype(jnp.bfloat16)
+            return c
+
+        lax.fori_loop(0, hidden // 128, hidden_tile, 0)
+        for qa in range(2):
+            far = pl.ds(pl.multiple_of((2 * qa + 1 - b) * lf, lf), lf)
+            msend[i, qa] = jnp.dot(
+                act[...], wd[:, far], preferred_element_type=jnp.float32
+            ).astype(jnp.bfloat16)
+        rsm(i).start()
+        for qa in range(2):
+            near = pl.ds(pl.multiple_of((2 * qa + b) * lf, lf), lf)
+            mine[qa] = jnp.dot(act[...], wd[:, near], preferred_element_type=jnp.float32)
+
+    over_group(0, spread)
+    for load in loads:
+        load.wait()
+
+    def step(i, c):
+        @pl.when(i + 1 < steps)
+        def _():
+            over_group(i + 1, spread)
+
+        over_group(i, relay)
+
+        @pl.when(i > 0)
+        def _():
+            reduce_mate(i - 1)
+
+        over_group(i, settle)
+        compute(i)
+
+        @pl.when(i > 0)
+        def _():
+            reduce_partner(i - 1)
+
+        return c
+
+    lax.fori_loop(0, steps, step, 0)
+    reduce_mate(steps - 1)
+    reduce_partner(steps - 1)
+    returned[me] = rsend[pl.ds(0, cap), :]
+
+    def finish(p):
+        agy(p).wait_send()
+        agm(p).wait_send()
+        agf(p).wait_send()
+
+        @pl.when(p > 0)
+        def _():
+            a2a(p).wait_send()
+            ret(p).wait_send()
+            ret(p).wait_recv()
+
+    each(0, n, finish)
+
+    def finish_group(i):
+        rsm(i).wait_send()
+        rsy(i).wait_send()
+
+    each(0, steps, finish_group)
+
+
+def expert_exchange(outgoing, expert_gate, expert_up, expert_down):
+    n, cap, lf = outgoing.shape
+    hidden = expert_gate.shape[2]
+    width = expert_gate.shape[1]
+    group = max(1, min(n, 256 // cap))
+    rows, steps = group * cap, n // group
+    bf, f32 = jnp.bfloat16, jnp.float32
+    dma = pltpu.SemaphoreType.DMA
+    return pl.pallas_call(
+        functools.partial(expert_kernel, n, group),
+        out_shape=jax.ShapeDtypeStruct((n, cap, lf), bf),
+        in_specs=[pl.BlockSpec(memory_space=pltpu.VMEM)]
+        + [pl.BlockSpec(memory_space=pl.ANY)] * 3,
+        out_specs=pl.BlockSpec(memory_space=pltpu.VMEM),
+        scratch_shapes=[
+            pltpu.VMEM((width, hidden), bf),
+            pltpu.VMEM((width, hidden), bf),
+            pltpu.VMEM((hidden, width), bf),
+            pltpu.VMEM((4, n * cap, lf), bf),
+            pltpu.VMEM((rows, hidden), bf),
+            pltpu.VMEM((steps, 2, rows, lf), bf),
+            pltpu.VMEM((steps, 2, rows, lf), bf),
+            pltpu.VMEM((2, rows, lf), f32),
+            pltpu.VMEM((steps, rows, lf), bf),
+            pltpu.VMEM((steps, rows, lf), bf),
+            pltpu.VMEM((rows, lf), f32),
+            pltpu.VMEM((n * cap, lf), bf),
+            dma((3,)),
+        ]
+        + [dma((n,))] * 8
+        + [dma((steps,))] * 4
+        + [dma((n,))] * 2,
+        compiler_params=pltpu.CompilerParams(
+            collective_id=0, has_side_effects=True, vmem_limit_bytes=48 * 1024 * 1024
+        ),
+        name="expert_exchange",
+    )(outgoing, expert_gate, expert_up, expert_down)
 
 
 def per_device(
@@ -76,23 +356,7 @@
     target, owners = slot_tables(routes, experts, capacity)
     padded = jnp.concatenate([normed, jnp.zeros((1, local_features), jnp.bfloat16)], axis=0)
     outgoing = padded[owners].reshape(experts, capacity, local_features)
-    slices_in = lax.all_to_all(outgoing, "sp", split_axis=0, concat_axis=0, tiled=True)
-    arrived = lax.all_gather(slices_in, "tp", axis=2, tiled=True)
-    expert_in = arrived.reshape(-1, model_width)
-    gate = jnp.dot(expert_in, expert_gate[0], preferred_element_type=jnp.float32)
-    upper = jnp.dot(expert_in, expert_up[0], preferred_element_type=jnp.float32)
-    act = (jax.nn.silu(gate) * upper).astype(jnp.bfloat16)
-    partial_out = jnp.dot(act, expert_down[0], preferred_element_type=jnp.float32)
-    summed = lax.psum_scatter(
-        partial_out.astype(jnp.bfloat16), "tp", scatter_dimension=1, tiled=True
-    )
-    returned = lax.all_to_all(
-        summed.reshape(experts, capacity, local_features),
-        "sp",
-        split_axis=0,
-        concat_axis=0,
-        tiled=True,
-    )
+    returned = expert_exchange(outgoing, expert_gate, expert_up, expert_down)
     picked = returned.reshape(experts * capacity, local_features)[target].astype(jnp.float32)
     picked = picked.reshape(tokens_here, 2, local_features)
     routed = jnp.sum(picked * route_weights[:, :, None], axis=1)

time: 213 us -> 126 us (0.59)
  waiting for transfers between devices: 104 us -> 0.01 us
  Pallas kernels: 0 us -> 80.9 us
  blocking collectives: 42 us -> 12.9 us
  matrix products: 19.7 us -> 1.38 us
  between operations: 13.6 us -> 0.19 us
  starting transfers between devices: 13.9 us -> 8.32 us
  local copies, waits for them, and re-layouts: 11.7 us -> 14.4 us
    pallas_call x0 -> x1, Pallas kernels: none -> 80.9 us  [expert_exchange(): pl.pallas_call(functools.partial(expert_kernel, n, group), out_shape=jax....]
    reduce_scatter x1 -> x0, waiting for transfers between devices: 44.6 us -> none  [per_device(): lax.psum_scatter(partial_out.astype(jnp.bfloat16), 'tp', scatter_dimensio...]
    all_gather x1 -> x0, waiting for transfers between devices: 33.6 us -> none  [per_device(): arrived = lax.all_gather(slices_in, 'tp', axis=2, tiled=True)]
    all_to_all x1 -> x0, blocking collectives: 29.1 us -> none  [per_device(): lax.all_to_all(outgoing, 'sp', split_axis=0, concat_axis=0, tiled=True)]
    all_to_all x1 -> x0, waiting for transfers between devices: 25.5 us -> none  [per_device(): lax.all_to_all(summed.reshape(experts, capacity, local_features), 'sp', s...]
    dot_general x3 -> x0, matrix products: 18.3 us -> none  [the longest x1 7.49 us: per_device(): upper = jnp.dot(expert_in, expert_up[0], preferred_element_type=jnp.float32)]
    all_to_all x1 -> x0, starting transfers between devices: 5.51 us -> none  [per_device(): lax.all_to_all(summed.reshape(experts, capacity, local_features), 'sp', s...]
    unnamed x14 -> x8, local copies, waits for them, and re-layouts: 0.97 us -> 3.66 us
  transfers between devices with their start and end apart: 5 -> 2, of which waited for: 3 -> 0; matrix products, arithmetic and copies ran while one was open for 4% -> 7% of each run, Pallas kernels for 0% -> 0%
where the time goes in v1:
time: 126 us
  Pallas kernels  80.9 us (64%)
  local copies, waits for them, and re-layouts  14.4 us (11%)
  blocking collectives  12.9 us (10%)
  starting transfers between devices  8.32 us (7%)
  other arithmetic  7.8 us (6%)
  matrix products  1.38 us (1%)
    pallas_call x1, Pallas kernels, expert_exchange(): pl.pallas_call(functools.partial(expert_kernel, n, group), out_shape=jax....  80.9 us
    ppermute x2, starting transfers between devices, from_behind(): return lax.ppermute(block, axis, route)  8.32 us
    psum x1, blocking collectives, per_device(): feature_total = lax.psum(jnp.sum(hidden_state * hidden_state, axis=1), 'tp')  7.1 us
    all_gather x1, blocking collectives, per_device(): lax.all_gather(mixed, 'tp', axis=1, tiled=True).astype(jnp.float32)  5.83 us
    gather x1, local copies, waits for them, and re-layouts, per_device(): outgoing = padded[owners].reshape(experts, capacity, local_features)  3.97 us
    unnamed x8, local copies, waits for them, and re-layouts  3.66 us
  transfers between devices with their start and end apart: 2, of which 0 were waited for; matrix products, arithmetic and copies ran while one was open for 7% of the time, Pallas kernels for 0%

profile of v1, /device:TPU:0, one launch (start us, length us, event | category | flops | bytes accessed | tf_op | source)
XLA Modules:
  0.0 125.9 jit_solution(14177848491400595794)
XLA Ops:
  0.0 0.0 copy-start
  0.0 0.0 copy-start.2
  0.0 0.7 convert_element_type.62
  0.7 0.1 slice.41
  0.8 4.9 %collective-permute-start.1 = (bf16[2]{0:T(256)(128)(2,1)S(1)}, bf16[2]{0:T(256)(128)(2,1)S(1)}, u32[]{:S(2)}, u32[]{:S(2)}) collective-permute-start(bf16[2]{0:T(256)(128)(2,1)S(1)} %slice.41), channel_id=1, source_target_pairs={{0,4},{4,8},{8,12},{12,16},{16,20},{20,24},{24,28},{1,5},{5,9},{9,... | collective-permute-start | bytes 20 | tf_op jit(solution)/shard_map/ppermute | solution.py:17
  5.7 0.9 multiply_convert_fusion.1
  6.6 3.5 %collective-permute-start = (bf16[2,128]{1,0:T(2,128)(2,1)S(1)}, bf16[2,128]{1,0:T(2,128)(2,1)S(1)}, u32[]{:S(2)}, u32[]{:S(2)}) collective-permute-start(bf16[2,128]{1,0:T(2,128)(2,1)S(1)} %slice.52), channel_id=1, source_target_pairs={{0,4},{4,8},{8,12},{12,16},{16,20},{20,24},{24,28},{1,5},{5,9},{9,... | collective-permute-start | bytes 1544 | tf_op jit(solution)/shard_map/ppermute | solution.py:17
  10.1 0.8 copy.17
  10.9 0.1 eq.37
  11.0 0.1 eq.33
  11.2 0.7 broadcast_multiply_fusion
  11.9 0.8 slice_bitcast_fusion.2
  12.7 1.1 reduce-window.6
  13.8 0.2 slice_reduce_fusion
  14.1 0.1 copy.16
  14.2 0.1 mul.144
  14.4 0.1 fusion.12
  14.5 2.4 %scatter_custom_fusion = s32[1024]{0:T(1024)S(1)} fusion(s32[512]{0:T(512)S(1)} %bitcast.22, s32[512]{0:T(512)S(1)} %add_select_fusion, s32[]{:T(128)} %constant.36.clone.1), kind=kCustom, calls=%fused_computation.42 | custom fusion | bytes 4100 | tf_op jit(solution)/shard_map/scatter | solution.py:30
  16.9 0.8 copy.19
  17.8 0.0 collective-permute-done.1
  17.8 0.1 pad_maximum_fusion
  17.8 0.8 compare_convert_fusion.1
  18.6 0.0 collective-permute-done
  18.6 1.0 fusion.8
  19.6 5.8 %all_gather.3 = bf16[256,512]{1,0:T(8,128)(2,1)S(1)} all-gather(bf16[256,128]{1,0:T(8,128)(2,1)S(1)} %fusion.8), channel_id=1, replica_groups=mesh['sp'=8,'tp'=4] {'tp'}, dimensions={1}, use_global_device_ids=true | all-gather | bytes 327680 | tf_op jit(solution)/shard_map/all_gather | solution.py:343
  25.4 0.1 fusion.2
  25.6 0.0 copy-done
  25.6 1.4 %multiply_reduce_fusion.1 = (f32[256]{0:T(256)S(1)}, f32[256,512]{1,0:T(8,128)S(1)}) fusion(f32[256]{0:T(256)S(1)} %add_rsqrt_fusion.1, bf16[512,512]{1,0:T(8,128)(2,1)S(1)} %copy-done, bf16[256,512]{1,0:T(8,128)(2,1)S(1)} %all_gather.3, f32[512]{0:T(512)} %param.20, bf16[256,512]{1,0:T(8,128)(2,1)} %param.14), kind=kOutput, calls=%fused_computation.12 | convolution fusion | flops 135266048 | bytes 1576960 | tf_op jit(solution)/shard_map/dot_general | solution.py:345
  27.0 7.1 %psum.7 = f32[256]{0:T(256)S(1)} all-reduce(f32[256]{0:T(256)S(1)} %get-tuple-element.10), channel_id=1, replica_groups=mesh['sp'=8,'tp'=4] {'tp'}, use_global_device_ids=true, to_apply=%region_2.0 | all-reduce | flops 256 | bytes 2048 | tf_op jit(solution)/shard_map/psum | solution.py:349
  34.1 0.0 copy-done.2
  34.1 0.1 multiply_convert_fusion
  34.2 4.0 %gather_fusion = bf16[1024,512]{1,0:T(8,128)(2,1)S(1)} fusion(bf16[257,512]{1,0:T(8,128)(2,1)S(1)} %concatenate.11, s32[1024]{0:T(1024)S(1)} %fusion.14), kind=kCustom, calls=%fused_computation | custom fusion | bytes 2101248 | tf_op jit(solution)/shard_map/gather | solution.py:358
  38.2 0.0 copy-start.1
  38.2 2.0 %copy-done.1 = bf16[1,2048,896]{2,1,0:T(8,128)(2,1)S(1)} copy-done((bf16[1,2048,896]{2,1,0:T(8,128)(2,1)S(1)}, bf16[1,2048,896]{2,1,0:T(8,128)(2,1)}, u32[]{:S(2)}) %copy-start.1) | copy-done | bytes 3670040
  40.3 80.9 %expert_exchange.1 = bf16[8,128,512]{2,1,0:T(8,128)(2,1)S(1)} custom-call(bf16[8,128,512]{2,1,0:T(8,128)(2,1)S(1)} %bitcast.20, bf16[1,2048,896]{2,1,0:T(8,128)(2,1)S(1)} %copy-done.1, bf16[1,2048,896]{2,1,0:T(8,128)(2,1)} %up_hbm.1, bf16[1,896,2048]{2,1,0:T(8,128)(2,1)} %down_hbm.1), custom_call_target="tpu_custom_call" | custom-call | tf_op jit(solution)/shard_map/expert_exchange/pallas_call | solution.py:279
  121.2 2.0 %gather_fusion.1 = bf16[512,512]{1,0:T(8,128)(2,1)S(1)} fusion(bf16[1024,512]{1,0:T(8,128)(2,1)S(1)} %bitcast.19, s32[1024]{0:T(1024)S(1)} %pad_clamp_fusion), kind=kCustom, calls=%fused_computation.1 | custom fusion | bytes 1050624 | tf_op jit(solution)/shard_map/gather | solution.py:360
  123.2 0.7 reshape.70
  123.8 1.3 %multiply_reduce_fusion = f32[256,512]{1,0:T(8,128)S(1)} fusion(f32[256,2,512]{2,1,0:T(2,128)S(1)} %reshape.70, f32[256,2]{1,0:T(8,128)S(1)} %copy.19), kind=kLoop, calls=%fused_computation.5 | loop fusion | flops 393216 | bytes 1574912 | tf_op jit(solution)/shard_map/reduce_sum | solution.py:362
  125.2 0.8 add_convert_fusion
  (12 shorter events, 0.1 us)
Async XLA Ops:
  0.0 25.6 %copy-start = (bf16[512,512]{1,0:T(8,128)(2,1)S(1)}, bf16[512,512]{1,0:T(8,128)(2,1)}, u32[]{:S(2)}) copy-start(bf16[512,512]{1,0:T(8,128)(2,1)} %param.21) | copy-start | bytes 1572868
  0.0 34.1 %copy-start.2 = (f32[512]{0:T(512)S(1)}, f32[512]{0:T(512)}, u32[]{:S(2)}) copy-start(f32[512]{0:T(512)} %param.22) | copy-start | bytes 6148
  0.8 16.9 %collective-permute-start.1 = (bf16[2]{0:T(256)(128)(2,1)S(1)}, bf16[2]{0:T(256)(128)(2,1)S(1)}, u32[]{:S(2)}, u32[]{:S(2)}) collective-permute-start(bf16[2]{0:T(256)(128)(2,1)S(1)} %slice.41), channel_id=1, source_target_pairs={{0,4},{4,8},{8,12},{12,16},{16,20},{20,24},{24,28},{1,5},{5,9},{9,... | collective-permute-start | bytes 20 | tf_op jit(solution)/shard_map/ppermute | solution.py:17
  6.6 12.0 %collective-permute-start = (bf16[2,128]{1,0:T(2,128)(2,1)S(1)}, bf16[2,128]{1,0:T(2,128)(2,1)S(1)}, u32[]{:S(2)}, u32[]{:S(2)}) collective-permute-start(bf16[2,128]{1,0:T(2,128)(2,1)S(1)} %slice.52), channel_id=1, source_target_pairs={{0,4},{4,8},{8,12},{12,16},{16,20},{20,24},{24,28},{1,5},{5,9},{9,... | collective-permute-start | bytes 1544 | tf_op jit(solution)/shard_map/ppermute | solution.py:17
  38.2 2.0 %copy-start.1 = (bf16[1,2048,896]{2,1,0:T(8,128)(2,1)S(1)}, bf16[1,2048,896]{2,1,0:T(8,128)(2,1)}, u32[]{:S(2)}) copy-start(bf16[1,2048,896]{2,1,0:T(8,128)(2,1)} %gate_hbm.1) | copy-start | bytes 11010052

commit v2 on v1

v2 whole, which is shorter than its diff:
```python
import functools

import jax
import jax.numpy as jnp
from jax import lax
from jax.experimental import pallas as pl
from jax.experimental.pallas import tpu as pltpu
from jax.sharding import PartitionSpec as P

EPS = 1e-06
MESH = pl.DeviceIdType.MESH


def layer_kernel(
    n,
    group,
    residual_hbm,
    conv_input,
    outer_gate,
    inner_gate,
    documents,
    conv_taps,
    mixer_gain,
    ow_hbm,
    ffn_gain,
    routes,
    route_weights,
    gate_hbm,
    up_hbm,
    down_hbm,
    layer_out,
    residual,
    ow,
    halo_conv,
    halo_inner,
    halo_docs,
    joined,
    joined_docs,
    mixbuf,
    totals,
    hidden,
    normed,
    outgoing,
    returned,
    wg,
    wu,
    wd,
    arrived,
    act,
    msend,
    mrecv,
    mine,
    ysend,
    yrecv,
    mine2,
    rsend,
    w_sem,
    a2a_s,
    a2a_r,
    agy_s,
    agy_r,
    agm_s,
    agm_r,
    agf_s,
    agf_r,
    rsm_s,
    rsm_r,
    rsy_s,
    rsy_r,
    ret_s,
    ret_r,
    halo_s,
    halo_r,
    mix_s,
    mix_r,
    tot_s,
    tot_r,
):
    me = lax.axis_index("sp")
    t = lax.axis_index("tp")
    a = t // 2
    b = t % 2
    mate = 2 * a + (1 - b)
    partner = 2 * (1 - a) + b
    across = 2 * (1 - a) + (1 - b)
    cap, lf = outgoing.shape[1], outgoing.shape[2]
    units = wg.shape[1]
    tokens = conv_input.shape[0]
    chans = conv_input.shape[1]
    rows = group * cap
    steps = n // group

    early = [
        pltpu.make_async_copy(ow_hbm, ow, w_sem.at[3]),
        pltpu.make_async_copy(residual_hbm, residual, w_sem.at[4]),
    ]
    loads = [
        pltpu.make_async_copy(gate_hbm.at[0], wg, w_sem.at[0]),
        pltpu.make_async_copy(up_hbm.at[0], wu, w_sem.at[1]),
        pltpu.make_async_copy(down_hbm.at[0], wd, w_sem.at[2]),
    ]
    for load in early + loads:
        load.start()

    barrier = pltpu.get_barrier_semaphore()

    def greet(p, c):
        pl.semaphore_signal(
            barrier, inc=1, device_id={"sp": (me + p) % n}, device_id_type=MESH
        )
        return c

    lax.fori_loop(1, n, greet, 0)
    for other in (mate, partner, across):
        pl.semaphore_signal(barrier, inc=1, device_id={"tp": other}, device_id_type=MESH)
    pl.semaphore_wait(barrier, n + 2)

    def remote(src, dst, s, r, dev):
        return pltpu.make_async_remote_copy(
            src_ref=src, dst_ref=dst, send_sem=s, recv_sem=r, device_id=dev, device_id_type=MESH
        )

    def span(p):
        return pl.ds(pl.multiple_of(p * cap, cap), cap)

    def span_g(i):
        return pl.ds(pl.multiple_of(i * rows, rows), rows)

    def a2a(p):
        return remote(
            outgoing.at[(me + p) % n],
            arrived.at[t, span(p)],
            a2a_s.at[p],
            a2a_r.at[p],
            {"sp": (me + p) % n},
        )

    def slab(p):
        return arrived.at[t, span(p)]

    def agy(p):
        return remote(slab(p), slab(p), agy_s.at[p], agy_r.at[p], {"tp": partner})

    def agm(p):
        return remote(slab(p), slab(p), agm_s.at[p], agm_r.at[p], {"tp": mate})

    def agf(p):
        piece = arrived.at[partner, span(p)]
        return remote(piece, piece, agf_s.at[p], agf_r.at[p], {"tp": mate})

    def rsm(i, h):
        return remote(
            msend.at[i, h], mrecv.at[i, h], rsm_s.at[i, h], rsm_r.at[i, h], {"tp": mate}
        )

    def rsy(p):
        return remote(
            ysend.at[span(p)], yrecv.at[span(p)], rsy_s.at[p], rsy_r.at[p], {"tp": partner}
        )

    def ret(p):
        return remote(
            rsend.at[span(p)],
            returned.at[span(me)],
            ret_s.at[p],
            ret_r.at[p],
            {"sp": (me + n - p) % n},
        )

    def each(low, high, f):
        def one(p, c):
            f(p)
            return c

        lax.fori_loop(low, high, one, 0)

    others = (mate, partner, across)

    @pl.when(me == 0)
    def _():
        halo_conv[...] = jnp.zeros_like(halo_conv)
        halo_inner[...] = jnp.zeros_like(halo_inner)
        halo_docs[...] = jnp.full_like(halo_docs, -1)

    def halo(j):
        last = pl.ds(tokens - 16, 16)
        src = (conv_input.at[last], inner_gate.at[last], documents)[j]
        dst = (halo_conv, halo_inner, halo_docs)[j]
        return remote(src, dst, halo_s.at[j], halo_r.at[j], {"sp": (me + 1) % n})

    @pl.when(me < n - 1)
    def _():
        for j in range(3):
            halo(j).start()

    f32, bf = jnp.float32, jnp.bfloat16
    row_id = lax.broadcasted_iota(jnp.int32, (tokens, tokens), 0)
    col_id = lax.broadcasted_iota(jnp.int32, (tokens, tokens), 1)
    eye = row_id == col_id

    def to_column(row):
        return jnp.sum(jnp.where(eye, row, 0.0), axis=1, keepdims=True)

    def to_row(column):
        return jnp.sum(jnp.where(eye, column, 0.0), axis=0, keepdims=True)

    expert_id = lax.broadcasted_iota(jnp.int32, (n, tokens), 0)
    hot = [(expert_id == routes[k : k + 1, :]).astype(f32) for k in range(2)]
    before = (row_id < col_id).astype(bf)
    counts = jnp.dot((hot[0] + hot[1]).astype(bf), before, preferred_element_type=f32)
    slots = [
        jnp.sum(hot[k] * (counts + (expert_id * cap).astype(f32)), axis=0, keepdims=True)
        for k in range(2)
    ]
    slot_rows = [s.astype(jnp.int32) for s in slots]
    slot_cols = [to_column(s).astype(jnp.int32) for s in slots]

    own = (inner_gate[...].astype(f32) * conv_input[...].astype(f32)).astype(bf).astype(f32)
    joined[pl.ds(16, tokens), :] = own
    doc_col = to_column(documents[...].astype(f32))
    joined_docs[pl.ds(16, tokens), :] = jnp.broadcast_to(doc_col, (tokens, chans))

    @pl.when(me > 0)
    def _():
        for j in range(3):
            halo(j).wait_recv()

    joined[pl.ds(0, 16), :] = (
        (halo_inner[...].astype(f32) * halo_conv[...].astype(f32)).astype(bf).astype(f32)
    )
    halo_col = to_column(halo_docs[...].astype(f32))
    joined_docs[pl.ds(0, 16), :] = jnp.broadcast_to(halo_col[tokens - 16 :, :], (16, chans))
    docs_here = joined_docs[pl.ds(16, tokens), :]
    same_one = (joined_docs[pl.ds(15, tokens), :] == docs_here).astype(f32)
    same_two = (joined_docs[pl.ds(14, tokens), :] == docs_here).astype(f32)
    conv_sum = (
        conv_taps[2:3, :] * own
        + conv_taps[1:2, :] * joined[pl.ds(15, tokens), :] * same_one
        + conv_taps[0:1, :] * joined[pl.ds(14, tokens), :] * same_two
    )
    mixbuf[t] = (outer_gate[...].astype(f32) * conv_sum).astype(bf)

    def mix(j):
        return remote(
            mixbuf.at[t], mixbuf.at[t], mix_s.at[j], mix_r.at[j], {"tp": others[j]}
        )

    for j in (1, 2, 0):
        mix(j).start()
    for load in early:
        load.wait()
    for j in range(3):
        mix(j).wait_recv()
    accum = None
    squares = None
    for q in range(4):
        piece = mixbuf[q].astype(f32)
        deep = slice(q * chans, (q + 1) * chans)
        scaled = (piece * mixer_gain[0:1, deep]).astype(bf)
        part = jnp.dot(scaled, ow[deep, :], preferred_element_type=f32)
        square = jnp.sum(piece * piece, axis=1, keepdims=True)
        accum = part if accum is None else accum + part
        squares = square if squares is None else squares + square
    mix_scale = lax.rsqrt(squares / (4 * chans) + EPS)
    hidden[...] = residual[...].astype(f32) + accum * mix_scale
    state = hidden[...]
    total = to_row(jnp.sum(state * state, axis=1, keepdims=True))
    totals[t] = jnp.broadcast_to(total, (8, tokens))

    def tot(j):
        return remote(
            totals.at[t], totals.at[t], tot_s.at[j], tot_r.at[j], {"tp": others[j]}
        )

    for j in (1, 2, 0):
        tot(j).start()
    for j in range(3):
        tot(j).wait_recv()
    feature_total = to_column((totals[0] + totals[1] + totals[2] + totals[3])[0:1, :])
    normed[...] = (
        hidden[...] * lax.rsqrt(feature_total / (4 * lf) + EPS) * ffn_gain[...]
    ).astype(bf)

    def pick_for(e):
        slot_id = lax.broadcasted_iota(jnp.int32, (cap, tokens), 0) + e * cap
        pick = (slot_id == slot_rows[0]) | (slot_id == slot_rows[1])
        return jnp.dot(
            pick.astype(f32).astype(bf), normed[...], preferred_element_type=f32
        ).astype(bf)

    def dispatch(p):
        e = (me + p) % n
        outgoing[e] = pick_for(e)
        a2a(p).start()

    each(1, n, dispatch)
    arrived[t, pl.ds(0, cap), :] = pick_for(me)

    def spread(p):
        @pl.when(p > 0)
        def _():
            a2a(p).wait_recv()

        agy(p).start()
        agm(p).start()

    def relay(p):
        agy(p).wait_recv()
        agf(p).start()

    def settle(p):
        agm(p).wait_recv()
        agf(p).wait_recv()

    def over_group(i, f):
        each(i * group, (i + 1) * group, f)

    def reduce_mate(i):
        rsm(i, 0).wait_recv()
        ysend[span_g(i), :] = (mine[0] + mrecv[i, 0].astype(jnp.float32)).astype(jnp.bfloat16)
        over_group(i, lambda p: rsy(p).start())
        rsm(i, 1).wait_recv()
        mine2[...] = mine[1] + mrecv[i, 1].astype(jnp.float32)

    def reduce_partner(i):
        def back(p):
            rsy(p).wait_recv()
            local = pl.ds(pl.multiple_of((p - i * group) * cap, cap), cap)
            rsend[span(p), :] = (
                mine2[local, :] + yrecv[span(p), :].astype(jnp.float32)
            ).astype(jnp.bfloat16)

            @pl.when(p > 0)
            def _():
                ret(p).start()

        over_group(i, back)

    def compute(i):
        def hidden_tile(j, c):
            cols = pl.ds(pl.multiple_of(j * 128, 128), 128)
            both = None
            for q in range(4):
                deep = slice(q * lf, (q + 1) * lf)
                w = jnp.concatenate([wg[deep, cols], wu[deep, cols]], axis=1)
                part = jnp.dot(arrived[q, span_g(i), :], w, preferred_element_type=jnp.float32)
                both = part if both is None else both + part
            g = both[:, :128]
            act[:, cols] = (g * jax.nn.sigmoid(g) * both[:, 128:]).astype(jnp.bfloat16)
            return c

        lax.fori_loop(0, units // 128, hidden_tile, 0)
        for h in range(2):
            qa = (1 - a) if h == 0 else a
            far = pl.ds(pl.multiple_of((2 * qa + 1 - b) * lf, lf), lf)
            near = pl.ds(pl.multiple_of((2 * qa + b) * lf, lf), lf)
            msend[i, h] = jnp.dot(
                act[...], wd[:, far], preferred_element_type=jnp.float32
            ).astype(jnp.bfloat16)
            rsm(i, h).start()
            mine[h] = jnp.dot(act[...], wd[:, near], preferred_element_type=jnp.float32)

    over_group(0, spread)
    if steps > 1:
        over_group(1, spread)
    for load in loads:
        load.wait()

    def step(i, c):
        over_group(i, relay)

        @pl.when(i > 0)
        def _():
            reduce_mate(i - 1)

        over_group(i, settle)

        @pl.when(i + 2 < steps)
        def _():
            over_group(i + 2, spread)

        compute(i)

        @pl.when(i > 0)
        def _():
            reduce_partner(i - 1)

        return c

    lax.fori_loop(0, steps, step, 0)
    reduce_mate(steps - 1)
    reduce_partner(steps - 1)
    returned[span(me), :] = rsend[pl.ds(0, cap), :]
    each(1, n, lambda p: ret(p).wait_recv())

    weight_cols = [to_column(route_weights[k : k + 1, :]) for k in range(2)]
    layer = hidden[...]
    for i in range(steps):
        here = returned[i * rows : (i + 1) * rows, :]
        slot_id = lax.broadcasted_iota(jnp.int32, (tokens, rows), 1) + i * rows
        for k in range(2):
            pick = (slot_id == slot_cols[k]).astype(f32).astype(bf)
            picked = jnp.dot(pick, here, preferred_element_type=f32)
            layer = layer + picked * weight_cols[k]
    layer_out[...] = layer.astype(bf)

    def finish(p):
        agy(p).wait_send()
        agm(p).wait_send()
        agf(p).wait_send()

        @pl.when(p > 0)
        def _():
            a2a(p).wait_send()
            ret(p).wait_send()

    each(0, n, finish)

    each(0, n, lambda p: rsy(p).wait_send())

    def finish_group(i):
        rsm(i, 0).wait_send()
        rsm(i, 1).wait_send()

    each(0, steps, finish_group)
    for j in range(3):
        mix(j).wait_send()
        tot(j).wait_send()

    @pl.when(me < n - 1)
    def _():
        for j in range(3):
            halo(j).wait_send()


def per_device(
    residual_in,
    conv_input,
    outer_gate,
    inner_gate,
    documents,
    conv_taps,
    mixer_gain,
    output_weight,
    ffn_gain,
    routes,
    route_weights,
    expert_gate,
    expert_up,
    expert_down,
):
    tokens, lf = residual_in.shape
    chans = conv_input.shape[1]
    n = lax.axis_size("sp") * expert_gate.shape[0]
    cap = 4 * tokens // n
    width, units = expert_gate.shape[1:]
    group = max(1, min(n, 256 // cap))
    rows, steps = group * cap, n // group
    bf, f32 = jnp.bfloat16, jnp.float32
    dma = pltpu.SemaphoreType.DMA
    vmem, hbm = pl.BlockSpec(memory_space=pltpu.VMEM), pl.BlockSpec(memory_space=pl.ANY)
    return pl.pallas_call(
        functools.partial(layer_kernel, n, group),
        out_shape=jax.ShapeDtypeStruct((tokens, lf), bf),
        in_specs=[hbm] + [vmem] * 6 + [hbm] + [vmem] * 3 + [hbm] * 3,
        out_specs=vmem,
        scratch_shapes=[
            pltpu.VMEM((tokens, lf), bf),
            pltpu.VMEM(output_weight.shape, bf),
            pltpu.VMEM((16, chans), bf),
            pltpu.VMEM((16, chans), bf),
            pltpu.VMEM((1, tokens), jnp.int32),
            pltpu.VMEM((tokens + 16, chans), f32),
            pltpu.VMEM((tokens + 16, chans), f32),
            pltpu.VMEM((4, tokens, chans), bf),
            pltpu.VMEM((4, 8, tokens), f32),
            pltpu.VMEM((tokens, lf), f32),
            pltpu.VMEM((tokens, lf), bf),
            pltpu.VMEM((n, cap, lf), bf),
            pltpu.VMEM((n * cap, lf), bf),
            pltpu.VMEM((width, units), bf),
            pltpu.VMEM((width, units), bf),
            pltpu.VMEM((units, width), bf),
            pltpu.VMEM((4, n * cap, lf), bf),
            pltpu.VMEM((rows, units), bf),
            pltpu.VMEM((steps, 2, rows, lf), bf),
            pltpu.VMEM((steps, 2, rows, lf), bf),
            pltpu.VMEM((2, rows, lf), f32),
            pltpu.VMEM((n * cap, lf), bf),
            pltpu.VMEM((n * cap, lf), bf),
            pltpu.VMEM((rows, lf), f32),
            pltpu.VMEM((n * cap, lf), bf),
            dma((5,)),
        ]
        + [dma((n,))] * 8
        + [dma((steps, 2))] * 2
        + [dma((n,))] * 4
        + [dma((3,))] * 6,
        compiler_params=pltpu.CompilerParams(
            collective_id=0, has_side_effects=True, vmem_limit_bytes=58 * 1024 * 1024
        ),
        name="layer",
    )(
        residual_in,
        conv_input,
        outer_gate,
        inner_gate,
        documents.reshape(1, tokens),
        conv_taps,
        mixer_gain.reshape(1, -1),
        output_weight,
        ffn_gain.reshape(1, -1),
        routes.T,
        route_weights.T,
        expert_gate,
        expert_up,
        expert_down,
    )


def solution(mesh):
    placed = (
        P("sp", "tp"),
        P("sp", "tp"),
        P("sp", "tp"),
        P("sp", "tp"),
        P("sp"),
        P(None, "tp"),
        P(),
        P(None, "tp"),
        P("tp"),
        P("sp", None),
        P("sp", None),
        P("sp", None, "tp"),
        P("sp", None, "tp"),
        P("sp", "tp", None),
    )
    return jax.shard_map(
        per_device, mesh=mesh, in_specs=placed, out_specs=P("sp", "tp"), check_vma=False
    )
```

time: 126 us -> 94.2 us (0.75)
  blocking collectives: 12.9 us -> 0 us
  local copies, waits for them, and re-layouts: 14.4 us -> 1.67 us
  Pallas kernels: 80.9 us -> 92.4 us
  starting transfers between devices: 8.32 us -> 0 us
  other arithmetic: 7.8 us -> 0 us
  matrix products: 1.38 us -> 0 us
    pallas_call x1, Pallas kernels: 80.9 us -> 92.4 us  [per_device(): pl.pallas_call(functools.partial(layer_kernel, n, group), out_shape=jax.S...]
    ppermute x2 -> x0, starting transfers between devices: 8.32 us -> none  [from_behind(): return lax.ppermute(block, axis, route)]
    psum x1 -> x0, blocking collectives: 7.1 us -> none  [per_device(): feature_total = lax.psum(jnp.sum(hidden_state * hidden_state, axis=1), 'tp')]
    gather x2 -> x0, local copies, waits for them, and re-layouts: 5.94 us -> none  [the longest x1 3.97 us: per_device(): outgoing = padded[owners].reshape(experts, capacity, local_features)]
    all_gather x1 -> x0, blocking collectives: 5.83 us -> none  [per_device(): lax.all_gather(mixed, 'tp', axis=1, tiled=True).astype(jnp.float32)]
    convert_element_type x8 -> x0, other arithmetic: 4.28 us -> none  [the longest x1 0.98 us: per_device(): mixed = (outer_gate.astype(jnp.float32) * conv_sum).astype(jnp.bfloat16)]
    scatter x1 -> x0, local copies, waits for them, and re-layouts: 2.45 us -> none  [slot_tables(): owners = jnp.full((experts * capacity,), tokens, jnp.int32).at[target].se...]
    unnamed x8 -> x1, local copies, waits for them, and re-layouts: 3.66 us -> 1.67 us
  transfers between devices with their start and end apart: 2 -> 0, of which waited for: 0 -> 0; matrix products, arithmetic and copies ran while one was open for 7% -> 0% of each run, Pallas kernels for 0% -> 0%
where the time goes in v2:
time: 94.2 us; the launch traced here: 94 us
  Pallas kernels  92.4 us (98%)
  local copies, waits for them, and re-layouts  1.67 us (2%)
    pallas_call x1, Pallas kernels, per_device(): pl.pallas_call(functools.partial(layer_kernel, n, group), out_shape=jax.S...  92.4 us

profile of v2, /device:TPU:0, one launch (start us, length us, event | category | flops | bytes accessed | tf_op | source)
XLA Modules:
  0.0 94.0 jit_solution(7834056206742489061)
XLA Ops:
  0.0 92.4 %layer.1 = bf16[256,512]{1,0:T(8,128)(2,1)} custom-call(bf16[256,512]{1,0:T(8,128)(2,1)} %residual_hbm.1, bf16[256,128]{1,0:T(8,128)(2,1)} %conv_input.1, bf16[256,128]{1,0:T(8,128)(2,1)} %outer_gate.1, bf16[256,128]{1,0:T(8,128)(2,1)} %inner_gate.1, s32[1,256]{1,0:T(1,128)} %bitcast.9, f32[3,128]{1,0:T(4,128)} %conv_taps.1, f32[1,512]{1,0:T(1,128)} %bitcast.5, ...), custom_call_target="tpu_custom_call" | custom-call | tf_op jit(solution)/shard_map/layer/pallas_call | solution.py:462
  92.4 1.7 %copy.16 = bf16[256,512]{1,0:T(8,128)(2,1)} copy(bf16[256,512]{1,0:T(8,128)(2,1)} %layer.1) | data formatting | bytes 524288

commit v3 on v2

--- a/solution.py
+++ b/solution.py
@@ -161,7 +161,7 @@
     def ret(p):
         return remote(
             rsend.at[span(p)],
-            returned.at[span(me)],
+            returned.at[span(p)],
             ret_s.at[p],
             ret_r.at[p],
             {"sp": (me + n - p) % n},
@@ -213,7 +213,11 @@
         for k in range(2)
     ]
     slot_rows = [s.astype(jnp.int32) for s in slots]
-    slot_cols = [to_column(s).astype(jnp.int32) for s in slots]
+    slot_cols = []
+    for s in slots:
+        near = s.astype(jnp.int32) - me * cap
+        near = jnp.where(near < 0, near + n * cap, near)
+        slot_cols.append(to_column(near.astype(f32)).astype(jnp.int32))
 
     own = (inner_gate[...].astype(f32) * conv_input[...].astype(f32)).astype(bf).astype(f32)
     joined[pl.ds(16, tokens), :] = own
@@ -293,14 +297,13 @@
         outgoing[e] = pick_for(e)
         a2a(p).start()
 
+    arrived[t, pl.ds(0, cap), :] = pick_for(me)
+    agy(0).start()
+    agm(0).start()
     each(1, n, dispatch)
-    arrived[t, pl.ds(0, cap), :] = pick_for(me)
 
     def spread(p):
-        @pl.when(p > 0)
-        def _():
-            a2a(p).wait_recv()
-
+        a2a(p).wait_recv()
         agy(p).start()
         agm(p).start()
 
@@ -337,19 +340,13 @@
         over_group(i, back)
 
     def compute(i):
-        def hidden_tile(j, c):
-            cols = pl.ds(pl.multiple_of(j * 128, 128), 128)
-            both = None
-            for q in range(4):
-                deep = slice(q * lf, (q + 1) * lf)
-                w = jnp.concatenate([wg[deep, cols], wu[deep, cols]], axis=1)
-                part = jnp.dot(arrived[q, span_g(i), :], w, preferred_element_type=jnp.float32)
-                both = part if both is None else both + part
+        whole = jnp.concatenate([arrived[q, span_g(i), :] for q in range(4)], axis=1)
+        for j in range(units // 128):
+            cols = slice(j * 128, (j + 1) * 128)
+            w = jnp.concatenate([wg[:, cols], wu[:, cols]], axis=1)
+            both = jnp.dot(whole, w, preferred_element_type=jnp.float32)
             g = both[:, :128]
             act[:, cols] = (g * jax.nn.sigmoid(g) * both[:, 128:]).astype(jnp.bfloat16)
-            return c
-
-        lax.fori_loop(0, units // 128, hidden_tile, 0)
         for h in range(2):
             qa = (1 - a) if h == 0 else a
             far = pl.ds(pl.multiple_of((2 * qa + 1 - b) * lf, lf), lf)
@@ -360,7 +357,7 @@
             rsm(i, h).start()
             mine[h] = jnp.dot(act[...], wd[:, near], preferred_element_type=jnp.float32)
 
-    over_group(0, spread)
+    each(1, group, spread)
     if steps > 1:
         over_group(1, spread)
     for load in loads:
@@ -389,20 +386,37 @@
 
     lax.fori_loop(0, steps, step, 0)
     reduce_mate(steps - 1)
-    reduce_partner(steps - 1)
-    returned[span(me), :] = rsend[pl.ds(0, cap), :]
-    each(1, n, lambda p: ret(p).wait_recv())
 
     weight_cols = [to_column(route_weights[k : k + 1, :]) for k in range(2)]
-    layer = hidden[...]
-    for i in range(steps):
-        here = returned[i * rows : (i + 1) * rows, :]
+
+    def combine(i):
+        def came(p):
+            @pl.when(p > 0)
+            def _():
+                ret(p).wait_recv()
+
+        over_group(i, came)
+        if i == 0:
+            here = jnp.concatenate(
+                [rsend[0:cap, :], returned[cap:rows, :]], axis=0
+            ) if group > 1 else rsend[0:cap, :]
+        else:
+            here = returned[i * rows : (i + 1) * rows, :]
         slot_id = lax.broadcasted_iota(jnp.int32, (tokens, rows), 1) + i * rows
+        total = hidden[...]
         for k in range(2):
             pick = (slot_id == slot_cols[k]).astype(f32).astype(bf)
             picked = jnp.dot(pick, here, preferred_element_type=f32)
-            layer = layer + picked * weight_cols[k]
-    layer_out[...] = layer.astype(bf)
+            total = total + picked * weight_cols[k]
+        return total
+
+    for i in range(steps - 2):
+        hidden[...] = combine(i)
+    reduce_partner(steps - 1)
+    for i in range(max(0, steps - 2), steps - 1):
+        hidden[...] = combine(i)
+    layer_out[...] = combine(steps - 1).astype(bf)
+
 
     def finish(p):
         agy(p).wait_send()

time: 94.2 us -> 93.5 us (level)
  no operation moved by 1% of the time
where the time goes in v3:
time: 93.5 us; the launch traced here: 93.3 us
  Pallas kernels  91.6 us (98%)
  local copies, waits for them, and re-layouts  1.67 us (2%)
    pallas_call x1, Pallas kernels, per_device(): pl.pallas_call(functools.partial(layer_kernel, n, group), out_shape=jax.S...  91.6 us

profile of v3, /device:TPU:0, one launch (start us, length us, event | category | flops | bytes accessed | tf_op | source)
XLA Modules:
  0.0 93.3 jit_solution(2461211645740285553)
XLA Ops:
  0.0 91.6 %layer.1 = bf16[256,512]{1,0:T(8,128)(2,1)} custom-call(bf16[256,512]{1,0:T(8,128)(2,1)} %residual_hbm.1, bf16[256,128]{1,0:T(8,128)(2,1)} %conv_input.1, bf16[256,128]{1,0:T(8,128)(2,1)} %outer_gate.1, bf16[256,128]{1,0:T(8,128)(2,1)} %inner_gate.1, s32[1,256]{1,0:T(1,128)} %bitcast.9, f32[3,128]{1,0:T(4,128)} %conv_taps.1, f32[1,512]{1,0:T(1,128)} %bitcast.5, ...), custom_call_target="tpu_custom_call" | custom-call | tf_op jit(solution)/shard_map/layer/pallas_call | solution.py:476
  91.6 1.7 %copy.16 = bf16[256,512]{1,0:T(8,128)(2,1)} copy(bf16[256,512]{1,0:T(8,128)(2,1)} %layer.1) | data formatting | bytes 524288
